TPU v7x, 512 devices: a whole 4x8x8 slice. The times are simulated.
512 devices in a mesh: row: 32 (over z, x), col: 16 (over y, core).
Axes of the slice: x: 4, y: 8, z: 8, core: 2. Of those that a mesh axis runs over, the one named last changes fastest.
Arguments:
- tokens: bfloat16 [32768, 2048], P('row'), may hold values from -136 to 136
- norm_gain: float32 [2048], replicated, may hold values from 0.1 to 1.9
- w_in: bfloat16 [2048, 1024], P(None, 'col'), may hold values from -0.125 to 0.125
- w_out: bfloat16 [1024, 2048], P(None, 'col'), may hold values from -0.1875 to 0.1875
Outputs:
- mixed_tokens: bfloat16 [32768, 2048], P('row', 'col')
All inputs are finite; a program needn't handle non-finite values.
Results may differ from a plain program's by a relative error of at most 0.013.
Values may be sent and summed in bfloat16 or wider, within the bound.
No kernel may reach another device: no remote copies, remote signals or barrier semaphores. Data moves between devices by JAX's collectives and lax.ppermute only.
A program may use at most 64 MiB of HBM per device.

v0:
```python
import math
import jax
import jax.numpy as jnp
from jax import lax
from jax.sharding import PartitionSpec as P

GROUP = 256
NORM_EPS = 1e-06


def in_one_piece(arrays, axis, split_dim, concat_dim, along):
    ends, at = ([], 0)
    for a in arrays[:-1]:
        at += a.shape[along]
        ends.append(at)
    both = jnp.concatenate(arrays, axis=along)
    return tuple(
        jnp.split(
            lax.all_to_all(both, axis, split_axis=split_dim, concat_axis=concat_dim, tiled=True),
            ends,
            axis=along,
        )
    )


def as_sent(array):

    def short(part):
        return part.astype(jnp.bfloat16) if part.dtype == jnp.float32 else part

    return jax.tree.map(short, array)


def rotation_table(first_index, second_index, spectral_magnitude, factor):
    phase = (first_index * second_index % spectral_magnitude).astype(jnp.float32) * (
        2.0 * math.pi / spectral_magnitude
    )
    return (jnp.cos(phase) * factor, jnp.sin(phase) * factor)


def twiddle(real_input_values, imag_in, freq_index, pos_index, spectral_magnitude):
    cosine, sine = rotation_table(freq_index, pos_index, spectral_magnitude, 1.0)
    return (
        real_input_values * cosine + imag_in * sine,
        imag_in * cosine - real_input_values * sine,
    )


def second_section(stacked, half):
    length_dev = stacked.shape[1]
    stride = min(length_dev, 512)
    positions = lax.broadcasted_iota(jnp.int32, (length_dev, stride), 0)
    real_blocks = []
    imag_blocks = []
    for offset in range(0, length_dev, stride):
        freqs = lax.broadcasted_iota(jnp.int32, (length_dev, stride), 1) + offset
        cosine, sine = rotation_table(positions, freqs, length_dev, 1.0)
        with_cos = jnp.dot(stacked, cosine, precision=lax.Precision.HIGH)
        with_sin = jnp.dot(stacked, sine, precision=lax.Precision.HIGH)
        real_blocks.append(with_cos[:half] + with_sin[half:])
        imag_blocks.append(with_cos[half:] - with_sin[:half])
    return (jnp.concatenate(real_blocks, 1), jnp.concatenate(imag_blocks, 1))


def reorder_positions(arrived):
    channels, row_count, _, block_len = arrived.shape
    return jnp.swapaxes(arrived.reshape(channels, row_count, block_len), 1, 2).reshape(
        channels, row_count * block_len
    )


def local(tokens, norm_gain, w_in, w_out):
    length_dev = tokens.shape[0]
    row_count = lax.axis_size("row")
    col_count = lax.axis_size("col")
    total_len = length_dev * row_count
    widened = tokens.astype(jnp.float32)
    inverse = lax.rsqrt(jnp.mean(widened * widened, axis=1, keepdims=True) + NORM_EPS)
    normed = (widened * inverse * norm_gain[None, :]).astype(jnp.bfloat16)
    projected = lax.dot_general(
        w_in, normed, (((0,), (1,)), ((), ())), preferred_element_type=jnp.float32
    ).astype(jnp.bfloat16)
    channels = projected.shape[0]
    block_len = length_dev // row_count
    small_cos, small_sin = rotation_table(
        lax.broadcasted_iota(jnp.int32, (row_count, row_count), 0),
        lax.broadcasted_iota(jnp.int32, (row_count, row_count), 1),
        row_count,
        1.0 / math.sqrt(total_len),
    )
    per_row = channels // row_count
    arrived = lax.all_to_all(
        projected.reshape(channels, 1, length_dev), "row", split_axis=0, concat_axis=1, tiled=True
    )
    values = arrived.astype(jnp.float32)
    real_one = jnp.einsum("ka,cab->ckb", small_cos, values, precision=lax.Precision.HIGH)
    imag_one = -jnp.einsum("ka,cab->ckb", small_sin, values, precision=lax.Precision.HIGH)
    freq_index = lax.broadcasted_iota(jnp.int32, (row_count, length_dev), 0)
    pos_index = lax.broadcasted_iota(jnp.int32, (row_count, length_dev), 1)
    real_two, imag_two = twiddle(real_one, imag_one, freq_index, pos_index, total_len)
    stacked = jnp.concatenate(
        [
            real_two.reshape(per_row * row_count, length_dev),
            imag_two.reshape(per_row * row_count, length_dev),
        ],
        0,
    )
    real_three, imag_three = second_section(stacked, per_row * row_count)
    shaped = (per_row, row_count, row_count, block_len)
    back_real, back_imag = tuple(
        (
            part.astype(jnp.float32)
            for part in in_one_piece(
                (
                    real_three.reshape(shaped).astype(jnp.bfloat16),
                    imag_three.reshape(shaped).astype(jnp.bfloat16),
                ),
                "row",
                2,
                0,
                1,
            )
        )
    )
    spec_real = reorder_positions(back_real)
    spec_imag = reorder_positions(back_imag)
    quarter = length_dev // col_count
    group_cosine_table, group_sine_table = rotation_table(
        lax.broadcasted_iota(jnp.int32, (GROUP, GROUP), 0),
        lax.broadcasted_iota(jnp.int32, (GROUP, GROUP), 1),
        GROUP,
        1.0 / math.sqrt(GROUP),
    )
    real_input_values = lax.all_to_all(
        as_sent(spec_real.reshape(channels, col_count, quarter)),
        "col",
        split_axis=1,
        concat_axis=0,
        tiled=True,
    )
    imag_in = lax.all_to_all(
        as_sent(spec_imag.reshape(channels, col_count, quarter)),
        "col",
        split_axis=1,
        concat_axis=0,
        tiled=True,
    )
    width_all = real_input_values.shape[0]
    item_count = real_input_values.shape[2]
    groups = width_all // GROUP
    real_by_group = real_input_values.reshape(groups, GROUP, item_count)
    imaginary_by_group = imag_in.reshape(groups, GROUP, item_count)
    merged_spectrum = jnp.einsum(
        "hz,azo->aho", group_cosine_table, real_by_group, precision=lax.Precision.HIGH
    )
    merged_spectrum = merged_spectrum + jnp.einsum(
        "hz,azo->aho", group_sine_table, imaginary_by_group, precision=lax.Precision.HIGH
    )
    result = merged_spectrum.reshape(width_all, 1, item_count).astype(jnp.bfloat16)
    portion = lax.all_gather(result, "col", axis=2, tiled=True)
    flat = portion.reshape(portion.shape[0], portion.shape[2])
    output = lax.dot_general(
        flat, w_out, (((0,), (0,)), ((), ())), preferred_element_type=jnp.float32
    )
    return output.astype(jnp.bfloat16)


def solution(mesh):
    placed = (P("row", None), P(), P(None, "col"), P(None, "col"))
    return jax.shard_map(
        local, mesh=mesh, in_specs=placed, out_specs=P("row", "col"), check_vma=False
    )
```

profile of v0, /device:TPU:1, one launch (start us, length us, event | category | flops | bytes accessed | tf_op | source)
XLA Modules:
  0.0 170.5 jit_solution(13047247857492114618)
XLA Ops:
  6.5 0.0 copy-start
  6.5 0.0 copy-start.1
  6.5 0.0 copy-start.2
  6.5 3.2 %fusion = f32[1024]{0:T(1024)S(1)} fusion(bf16[1024,2048]{1,0:T(8,128)(2,1)} %param.4), kind=kLoop, calls=%fused_computation.2 | loop fusion | flops 6290432 | bytes 4198400 | tf_op jit(solution)/shard_map/reduce_sum | solution.py:78
  9.8 0.3 copy-done.1
  10.0 0.0 copy-done.2
  10.0 2.4 %fusion.38 = bf16[64,1,1024]{2,0,1:T(8,128)(2,1)S(1)} fusion(bf16[2048,64]{0,1:T(8,128)(2,1)} %param.6, bf16[1024,2048]{1,0:T(8,128)(2,1)S(1)} %copy-done.1, f32[2048]{0:T(1024)S(1)} %copy-done.2, f32[1024]{0:T(1024)S(1)} %add_rsqrt_fusion), kind=kOutput, calls=%fused_computation.44 | convolution fusion | flops 276889600 | bytes 4599808 | tf_op jit(solution)/shard_map/dot_general | solution.py:80
  12.4 0.5 broadcast.165
  13.0 0.7 reduce.1
  13.6 0.7 reshape.90
  14.3 13.9 %all-to-all-start = ((bf16[32,2,1024]{2,1,0:T(2,128)(2,1)}), bf16[32,2,1024]{2,1,0:T(2,128)(2,1)S(1)}, u32[]{:S(2)}, u32[]{:S(2)}) async-start(bf16[32,2,1024]{2,1,0:T(2,128)(2,1)} %reshape.90), calls=%async_computation | async-start | bytes 262144 | tf_op jit(solution)/shard_map/all_to_all | solution.py:92
  28.2 0.5 fusion.78
  28.8 8.6 %all-to-all-done = bf16[32,2,1024]{2,1,0:T(2,128)(2,1)S(1)} async-done(((bf16[32,2,1024]{2,1,0:T(2,128)(2,1)}), bf16[32,2,1024]{2,1,0:T(2,128)(2,1)S(1)}, u32[]{:S(2)}, u32[]{:S(2)}) %all-to-all-start) | async-done | bytes 131104 | tf_op jit(solution)/shard_map/all_to_all | solution.py:92
  37.4 0.1 reshape.91
  37.5 0.7 reduce
  38.3 0.1 all_to_all.49
  38.3 0.3 convolution_bitcast_fusion
  38.6 0.3 multiply_add_fusion
  38.9 8.7 %fusion.21 = f32[128,512]{1,0:T(8,128)S(1)} fusion(f32[64,1024]{1,0:T(8,128)S(1)} %bitcast.98, f32[64,1024]{1,0:T(8,128)S(1)} %bitcast.94), kind=kOutput, calls=%fused_computation.28 | convolution fusion | flops 410124288 | bytes 786432 | tf_op jit(solution)/shard_map/dot_general | solution.py:59
  47.6 8.6 %fusion.17 = f32[128,512]{1,0:T(8,128)S(1)} fusion(s32[512]{0:T(512)S(1)} %iota_add_fusion, f32[64,1024]{1,0:T(8,128)S(1)} %bitcast.99, f32[64,1024]{1,0:T(8,128)S(1)} %bitcast.95), kind=kOutput, calls=%fused_computation.24 | convolution fusion | flops 410124288 | bytes 788480 | tf_op jit(solution)/shard_map/dot_general | solution.py:58
  56.2 8.9 %fusion.15 = f32[128,512]{1,0:T(8,128)S(1)} fusion(s32[512]{0:T(512)S(1)} %iota_add_fusion, f32[64,1024]{1,0:T(8,128)S(1)} %bitcast.100, f32[64,1024]{1,0:T(8,128)S(1)} %bitcast.96), kind=kOutput, calls=%fused_computation.22 | convolution fusion | flops 410124288 | bytes 788480 | tf_op jit(solution)/shard_map/dot_general | solution.py:59
  65.1 8.6 %fusion.23 = f32[128,512]{1,0:T(8,128)S(1)} fusion(f32[64,1024]{1,0:T(8,128)S(1)} %bitcast.101, f32[64,1024]{1,0:T(8,128)S(1)} %bitcast.97), kind=kOutput, calls=%fused_computation.30 | convolution fusion | flops 410124288 | bytes 786432 | tf_op jit(solution)/shard_map/dot_general | solution.py:58
  73.9 0.4 convert_element_type.108
  74.2 0.7 copy.35
  74.9 0.4 convert_element_type.107
  75.3 0.7 copy.34
  75.9 0.3 fusion.136
  76.2 0.4 reshape.92
  76.6 13.7 %all_to_all.66 = bf16[32,2,2048]{2,1,0:T(2,128)(2,1)S(1)} all-to-all(bf16[32,2,2048]{2,1,0:T(2,128)(2,1)S(1)} %reshape.92), channel_id=1, replica_groups=mesh['row'=32,'col'=16] {'row'}, dimensions={0} | all-to-all | bytes 524288 | tf_op jit(solution)/shard_map/all_to_all | solution.py:19
  90.3 0.4 reshape.93
  90.7 0.2 slice_bitcast_fusion
  90.9 0.6 copy.41
  91.5 0.9 reshape.96
  92.4 10.9 %all-to-all-start.3 = ((bf16[16,2,2048]{2,1,0:T(2,128)(2,1)}), bf16[16,2,2048]{2,1,0:T(2,128)(2,1)S(1)}, u32[]{:S(2)}, u32[]{:S(2)}) async-start(bf16[16,2,2048]{2,1,0:T(2,128)(2,1)} %reshape.96), calls=%async_computation.3 | async-start | bytes 262144 | tf_op jit(solution)/shard_map/all_to_all | solution.py:141
  103.3 0.6 copy.37
  103.9 0.9 reshape.94
  104.8 7.4 %all-to-all-done.3 = bf16[16,2,2048]{2,1,0:T(2,128)(2,1)S(1)} async-done(((bf16[16,2,2048]{2,1,0:T(2,128)(2,1)}), bf16[16,2,2048]{2,1,0:T(2,128)(2,1)S(1)}, u32[]{:S(2)}, u32[]{:S(2)}) %all-to-all-start.3) | async-done | bytes 131104 | tf_op jit(solution)/shard_map/all_to_all | solution.py:141
  112.2 3.4 %all-to-all-start.2 = ((bf16[16,2,2048]{2,1,0:T(2,128)(2,1)}), bf16[16,2,2048]{2,1,0:T(2,128)(2,1)S(1)}, u32[]{:S(2)}, u32[]{:S(2)}) async-start(bf16[16,2,2048]{2,1,0:T(2,128)(2,1)} %reshape.94), calls=%async_computation.2 | async-start | bytes 262144 | tf_op jit(solution)/shard_map/all_to_all | solution.py:134
  115.6 0.0 all-gather.2.cloned.1.call-start
  115.6 0.2 reshape.97
  115.9 0.2 copy.42
  116.1 0.2 reshape.83
  116.3 8.2 %all-to-all-done.2 = bf16[16,2,2048]{2,1,0:T(2,128)(2,1)S(1)} async-done(((bf16[16,2,2048]{2,1,0:T(2,128)(2,1)}), bf16[16,2,2048]{2,1,0:T(2,128)(2,1)S(1)}, u32[]{:S(2)}, u32[]{:S(2)}) %all-to-all-start.2) | async-done | bytes 131104 | tf_op jit(solution)/shard_map/all_to_all | solution.py:134
  124.5 0.2 reshape.95
  124.8 0.2 copy.38
  125.0 0.2 reshape.82
  125.2 1.2 fusion.49
  126.4 1.2 fusion.37
  127.6 0.1 copy.44
  127.7 0.7 convert_element_type.118
  128.4 0.0 all-gather.2.cloned.1.call-update
  128.5 32.2 %all-gather.2.cloned.1.call-done = bf16[1024,1,1024]{0,2,1:T(8,128)(2,1)} async-done(((bf16[1024,1,64]{0,2,1:T(8,128)(2,1)}), bf16[1024,1,1024]{0,2,1:T(8,128)(2,1)}) %all-gather.2.cloned.1.call-update) | async-done | bytes 2097168 | tf_op jit(solution)/shard_map/all_gather | solution.py:160
  160.7 0.0 copy-done
  160.7 3.0 %fusion.29 = bf16[1024,128]{1,0:T(8,128)(2,1)} fusion(bf16[1024,128]{1,0:T(8,128)(2,1)S(1)} %copy-done, bf16[1024,1,1024]{0,2,1:T(8,128)(2,1)} %all-gather.2.cloned.1.call-done), kind=kOutput, calls=%fused_computation.36 | convolution fusion | flops 268566528 | bytes 2621440 | tf_op jit(solution)/shard_map/dot_general | solution.py:162
  (10 shorter events, 0.2 us)
Async XLA Ops:
  6.5 154.2 %copy-start = (bf16[1024,128]{1,0:T(8,128)(2,1)S(1)}, bf16[1024,128]{1,0:T(8,128)(2,1)}, u32[]{:S(2)}) copy-start(bf16[1024,128]{1,0:T(8,128)(2,1)} %param.7) | copy-start | bytes 786436
  6.5 3.5 %copy-start.1 = (bf16[1024,2048]{1,0:T(8,128)(2,1)S(1)}, bf16[1024,2048]{1,0:T(8,128)(2,1)}, u32[]{:S(2)}) copy-start(bf16[1024,2048]{1,0:T(8,128)(2,1)} %param.4) | copy-start | bytes 12582916
  6.5 3.5 %copy-start.2 = (f32[2048]{0:T(1024)S(1)}, f32[2048]{0:T(1024)}, u32[]{:S(2)}) copy-start(f32[2048]{0:T(1024)} %param.5) | copy-start | bytes 24580
  14.3 23.1 %all-to-all-start = ((bf16[32,2,1024]{2,1,0:T(2,128)(2,1)}), bf16[32,2,1024]{2,1,0:T(2,128)(2,1)S(1)}, u32[]{:S(2)}, u32[]{:S(2)}) async-start(bf16[32,2,1024]{2,1,0:T(2,128)(2,1)} %reshape.90), calls=%async_computation | async-start | bytes 262144 | tf_op jit(solution)/shard_map/all_to_all | solution.py:92
  92.4 19.8 %all-to-all-start.3 = ((bf16[16,2,2048]{2,1,0:T(2,128)(2,1)}), bf16[16,2,2048]{2,1,0:T(2,128)(2,1)S(1)}, u32[]{:S(2)}, u32[]{:S(2)}) async-start(bf16[16,2,2048]{2,1,0:T(2,128)(2,1)} %reshape.96), calls=%async_computation.3 | async-start | bytes 262144 | tf_op jit(solution)/shard_map/all_to_all | solution.py:141
  112.2 12.3 %all-to-all-start.2 = ((bf16[16,2,2048]{2,1,0:T(2,128)(2,1)}), bf16[16,2,2048]{2,1,0:T(2,128)(2,1)S(1)}, u32[]{:S(2)}, u32[]{:S(2)}) async-start(bf16[16,2,2048]{2,1,0:T(2,128)(2,1)} %reshape.94), calls=%async_computation.2 | async-start | bytes 262144 | tf_op jit(solution)/shard_map/all_to_all | solution.py:134
  115.6 45.1 %all-gather.2.cloned.1.call-start = ((), (), s32[]{:S(2)}) async-start(), calls=%async_computation.4 | async-start | bytes 2228224 | tf_op jit(solution)/shard_map/all_gather | solution.py:160
Sparse Core Ops, SparseCore 0:
  128.6 32.0 all-gather.1
where the time goes:
time: 171 us
  waiting for transfers between devices  56.5 us (33%)
  matrix products  43.2 us (25%)
  starting transfers between devices  28.2 us (16%)
  blocking collectives  13.7 us (8%)
  between operations  13.7 us (8%)
  local copies, waits for them, and re-layouts  9.71 us (6%)
  other arithmetic  5.56 us (3%)
    all_gather x1, waiting for transfers between devices, local(): portion = lax.all_gather(result, 'col', axis=2, tiled=True)  32.2 us
    dot_general x2, matrix products, second_section(): with_sin = jnp.dot(stacked, sine, precision=lax.Precision.HIGH)  17.6 us
    dot_general x2, matrix products, second_section(): with_cos = jnp.dot(stacked, cosine, precision=lax.Precision.HIGH)  17.2 us
    all_to_all x1, starting transfers between devices, local(): lax.all_to_all(projected.reshape(channels, 1, length_dev), 'row', split_a...  13.9 us
    all_to_all x1, blocking collectives, in_one_piece(): lax.all_to_all(both, axis, split_axis=split_dim, concat_axis=concat_dim,...  13.7 us
    all_to_all x1, starting transfers between devices, local(): lax.all_to_all(as_sent(spec_imag.reshape(channels, col_count, quarter)),...  10.9 us
    all_to_all x1, waiting for transfers between devices, local(): lax.all_to_all(projected.reshape(channels, 1, length_dev), 'row', split_a...  8.62 us
    all_to_all x1, waiting for transfers between devices, local(): lax.all_to_all(as_sent(spec_real.reshape(channels, col_count, quarter)),...  8.24 us
  transfers between devices with their start and end apart: 4, of which 4 were waited for; matrix products, arithmetic and copies ran while one was open for 2% of the time, Pallas kernels for 0%

commit v1 on v0

--- a/solution.py
+++ b/solution.py
@@ -6,6 +6,12 @@
 
 GROUP = 256
 NORM_EPS = 1e-06
+
+
+def gathered_along(x, mesh_axis, along):
+    terms = lax.all_gather(x, mesh_axis, axis=0, tiled=False)
+    whole = jnp.concatenate(terms, axis=along)
+    return whole
 
 
 def in_one_piece(arrays, axis, split_dim, concat_dim, along):
@@ -157,7 +163,7 @@
         "hz,azo->aho", group_sine_table, imaginary_by_group, precision=lax.Precision.HIGH
     )
     result = merged_spectrum.reshape(width_all, 1, item_count).astype(jnp.bfloat16)
-    portion = lax.all_gather(result, "col", axis=2, tiled=True)
+    portion = gathered_along(result, "col", 2)
     flat = portion.reshape(portion.shape[0], portion.shape[2])
     output = lax.dot_general(
         flat, w_out, (((0,), (0,)), ((), ())), preferred_element_type=jnp.float32

time: 171 us -> 171 us (level)
  no operation moved by 1% of the time
where the time goes in v1:
time: 171 us
  waiting for transfers between devices  56.5 us (33%)
  matrix products  43.2 us (25%)
  starting transfers between devices  28.2 us (16%)
  blocking collectives  13.7 us (8%)
  between operations  13.7 us (8%)
  local copies, waits for them, and re-layouts  9.71 us (6%)
  other arithmetic  5.56 us (3%)
    all_gather x1, waiting for transfers between devices, gathered_along(): terms = lax.all_gather(x, mesh_axis, axis=0, tiled=False)  32.2 us
    dot_general x2, matrix products, second_section(): with_sin = jnp.dot(stacked, sine, precision=lax.Precision.HIGH)  17.6 us
    dot_general x2, matrix products, second_section(): with_cos = jnp.dot(stacked, cosine, precision=lax.Precision.HIGH)  17.2 us
    all_to_all x1, starting transfers between devices, local(): lax.all_to_all(projected.reshape(channels, 1, length_dev), 'row', split_a...  13.9 us
    all_to_all x1, blocking collectives, in_one_piece(): lax.all_to_all(both, axis, split_axis=split_dim, concat_axis=concat_dim,...  13.7 us
    all_to_all x1, starting transfers between devices, local(): lax.all_to_all(as_sent(spec_imag.reshape(channels, col_count, quarter)),...  10.9 us
    all_to_all x1, waiting for transfers between devices, local(): lax.all_to_all(projected.reshape(channels, 1, length_dev), 'row', split_a...  8.62 us
    all_to_all x1, waiting for transfers between devices, local(): lax.all_to_all(as_sent(spec_real.reshape(channels, col_count, quarter)),...  8.24 us
  transfers between devices with their start and end apart: 4, of which 4 were waited for; matrix products, arithmetic and copies ran while one was open for 2% of the time, Pallas kernels for 0%

profile of v1, /device:TPU:1, one launch (start us, length us, event | category | flops | bytes accessed | tf_op | source)
XLA Modules:
  0.0 170.5 jit_solution(7468568820771376894)
XLA Ops:
  6.5 0.0 copy-start
  6.5 0.0 copy-start.1
  6.5 0.0 copy-start.2
  6.5 3.2 %fusion = f32[1024]{0:T(1024)S(1)} fusion(bf16[1024,2048]{1,0:T(8,128)(2,1)} %param.4), kind=kLoop, calls=%fused_computation.2 | loop fusion | flops 6290432 | bytes 4198400 | tf_op jit(solution)/shard_map/reduce_sum | solution.py:84
  9.8 0.3 copy-done.1
  10.0 0.0 copy-done.2
  10.0 2.4 %fusion.33 = bf16[64,1,1024]{2,0,1:T(8,128)(2,1)S(1)} fusion(bf16[2048,64]{0,1:T(8,128)(2,1)} %param.6, bf16[1024,2048]{1,0:T(8,128)(2,1)S(1)} %copy-done.1, f32[2048]{0:T(1024)S(1)} %copy-done.2, f32[1024]{0:T(1024)S(1)} %add_rsqrt_fusion), kind=kOutput, calls=%fused_computation.42 | convolution fusion | flops 276889600 | bytes 4599808 | tf_op jit(solution)/shard_map/dot_general | solution.py:86
  12.4 0.5 broadcast.165
  13.0 0.7 reduce.1
  13.6 0.7 reshape.91
  14.3 13.9 %all-to-all-start = ((bf16[32,2,1024]{2,1,0:T(2,128)(2,1)}), bf16[32,2,1024]{2,1,0:T(2,128)(2,1)S(1)}, u32[]{:S(2)}, u32[]{:S(2)}) async-start(bf16[32,2,1024]{2,1,0:T(2,128)(2,1)} %reshape.91), calls=%async_computation | async-start | bytes 262144 | tf_op jit(solution)/shard_map/all_to_all | solution.py:98
  28.2 0.5 fusion.73
  28.8 8.6 %all-to-all-done = bf16[32,2,1024]{2,1,0:T(2,128)(2,1)S(1)} async-done(((bf16[32,2,1024]{2,1,0:T(2,128)(2,1)}), bf16[32,2,1024]{2,1,0:T(2,128)(2,1)S(1)}, u32[]{:S(2)}, u32[]{:S(2)}) %all-to-all-start) | async-done | bytes 131104 | tf_op jit(solution)/shard_map/all_to_all | solution.py:98
  37.4 0.1 reshape.92
  37.5 0.7 reduce
  38.3 0.1 all_to_all.49
  38.3 0.3 convolution_bitcast_fusion
  38.6 0.3 multiply_add_fusion
  38.9 8.7 %fusion.19 = f32[128,512]{1,0:T(8,128)S(1)} fusion(f32[64,1024]{1,0:T(8,128)S(1)} %bitcast.99, f32[64,1024]{1,0:T(8,128)S(1)} %bitcast.95), kind=kOutput, calls=%fused_computation.26 | convolution fusion | flops 410124288 | bytes 786432 | tf_op jit(solution)/shard_map/dot_general | solution.py:65
  47.6 8.6 %fusion.15 = f32[128,512]{1,0:T(8,128)S(1)} fusion(s32[512]{0:T(512)S(1)} %iota_add_fusion, f32[64,1024]{1,0:T(8,128)S(1)} %bitcast.100, f32[64,1024]{1,0:T(8,128)S(1)} %bitcast.96), kind=kOutput, calls=%fused_computation.22 | convolution fusion | flops 410124288 | bytes 788480 | tf_op jit(solution)/shard_map/dot_general | solution.py:64
  56.2 8.9 %fusion.13 = f32[128,512]{1,0:T(8,128)S(1)} fusion(s32[512]{0:T(512)S(1)} %iota_add_fusion, f32[64,1024]{1,0:T(8,128)S(1)} %bitcast.101, f32[64,1024]{1,0:T(8,128)S(1)} %bitcast.97), kind=kOutput, calls=%fused_computation.20 | convolution fusion | flops 410124288 | bytes 788480 | tf_op jit(solution)/shard_map/dot_general | solution.py:65
  65.1 8.6 %fusion.21 = f32[128,512]{1,0:T(8,128)S(1)} fusion(f32[64,1024]{1,0:T(8,128)S(1)} %bitcast.102, f32[64,1024]{1,0:T(8,128)S(1)} %bitcast.98), kind=kOutput, calls=%fused_computation.28 | convolution fusion | flops 410124288 | bytes 786432 | tf_op jit(solution)/shard_map/dot_general | solution.py:64
  73.9 0.4 convert_element_type.109
  74.2 0.7 copy.34
  74.9 0.4 convert_element_type.108
  75.3 0.7 copy.33
  75.9 0.3 fusion.131
  76.2 0.4 reshape.93
  76.6 13.7 %all_to_all.66 = bf16[32,2,2048]{2,1,0:T(2,128)(2,1)S(1)} all-to-all(bf16[32,2,2048]{2,1,0:T(2,128)(2,1)S(1)} %reshape.93), channel_id=1, replica_groups=mesh['row'=32,'col'=16] {'row'}, dimensions={0} | all-to-all | bytes 524288 | tf_op jit(solution)/shard_map/all_to_all | solution.py:25
  90.3 0.4 reshape.94
  90.7 0.2 slice_bitcast_fusion
  90.9 0.6 copy.40
  91.5 0.9 reshape.97
  92.4 10.9 %all-to-all-start.3 = ((bf16[16,2,2048]{2,1,0:T(2,128)(2,1)}), bf16[16,2,2048]{2,1,0:T(2,128)(2,1)S(1)}, u32[]{:S(2)}, u32[]{:S(2)}) async-start(bf16[16,2,2048]{2,1,0:T(2,128)(2,1)} %reshape.97), calls=%async_computation.3 | async-start | bytes 262144 | tf_op jit(solution)/shard_map/all_to_all | solution.py:147
  103.3 0.6 copy.36
  103.9 0.9 reshape.95
  104.8 7.4 %all-to-all-done.3 = bf16[16,2,2048]{2,1,0:T(2,128)(2,1)S(1)} async-done(((bf16[16,2,2048]{2,1,0:T(2,128)(2,1)}), bf16[16,2,2048]{2,1,0:T(2,128)(2,1)S(1)}, u32[]{:S(2)}, u32[]{:S(2)}) %all-to-all-start.3) | async-done | bytes 131104 | tf_op jit(solution)/shard_map/all_to_all | solution.py:147
  112.2 3.4 %all-to-all-start.2 = ((bf16[16,2,2048]{2,1,0:T(2,128)(2,1)}), bf16[16,2,2048]{2,1,0:T(2,128)(2,1)S(1)}, u32[]{:S(2)}, u32[]{:S(2)}) async-start(bf16[16,2,2048]{2,1,0:T(2,128)(2,1)} %reshape.95), calls=%async_computation.2 | async-start | bytes 262144 | tf_op jit(solution)/shard_map/all_to_all | solution.py:140
  115.6 0.0 all-gather.2.cloned.1.call-start
  115.6 0.2 reshape.98
  115.9 0.2 copy.41
  116.1 0.2 reshape.84
  116.3 8.2 %all-to-all-done.2 = bf16[16,2,2048]{2,1,0:T(2,128)(2,1)S(1)} async-done(((bf16[16,2,2048]{2,1,0:T(2,128)(2,1)}), bf16[16,2,2048]{2,1,0:T(2,128)(2,1)S(1)}, u32[]{:S(2)}, u32[]{:S(2)}) %all-to-all-start.2) | async-done | bytes 131104 | tf_op jit(solution)/shard_map/all_to_all | solution.py:140
  124.5 0.2 reshape.96
  124.8 0.2 copy.37
  125.0 0.2 reshape.83
  125.2 1.2 fusion.44
  126.4 1.2 fusion.32
  127.6 0.1 copy.43
  127.7 0.7 convert_element_type.119
  128.4 0.0 all-gather.2.cloned.1.call-update
  128.5 32.2 %all-gather.2.cloned.1.call-done = bf16[16,1024,1,64]{1,3,2,0:T(8,128)(2,1)} async-done(((bf16[1,1024,1,64]{1,3,2,0:T(8,128)(2,1)}), bf16[16,1024,1,64]{1,3,2,0:T(8,128)(2,1)}) %all-gather.2.cloned.1.call-update) | async-done | bytes 2097168 | tf_op jit(solution)/shard_map/all_gather | solution.py:12
  160.7 0.0 copy-done
  160.7 3.0 %convolution_convert_fusion = bf16[1024,128]{1,0:T(8,128)(2,1)} fusion(bf16[1024,1024]{0,1:T(8,128)(2,1)} %bitcast.92, bf16[1024,128]{1,0:T(8,128)(2,1)S(1)} %copy-done), kind=kOutput, calls=%fused_computation.34 | convolution fusion | flops 268566528 | bytes 2621440 | tf_op jit(solution)/shard_map/dot_general | solution.py:168
  (10 shorter events, 0.2 us)
Async XLA Ops:
  6.5 154.2 %copy-start = (bf16[1024,128]{1,0:T(8,128)(2,1)S(1)}, bf16[1024,128]{1,0:T(8,128)(2,1)}, u32[]{:S(2)}) copy-start(bf16[1024,128]{1,0:T(8,128)(2,1)} %param.7) | copy-start | bytes 786436
  6.5 3.5 %copy-start.1 = (bf16[1024,2048]{1,0:T(8,128)(2,1)S(1)}, bf16[1024,2048]{1,0:T(8,128)(2,1)}, u32[]{:S(2)}) copy-start(bf16[1024,2048]{1,0:T(8,128)(2,1)} %param.4) | copy-start | bytes 12582916
  6.5 3.5 %copy-start.2 = (f32[2048]{0:T(1024)S(1)}, f32[2048]{0:T(1024)}, u32[]{:S(2)}) copy-start(f32[2048]{0:T(1024)} %param.5) | copy-start | bytes 24580
  14.3 23.1 %all-to-all-start = ((bf16[32,2,1024]{2,1,0:T(2,128)(2,1)}), bf16[32,2,1024]{2,1,0:T(2,128)(2,1)S(1)}, u32[]{:S(2)}, u32[]{:S(2)}) async-start(bf16[32,2,1024]{2,1,0:T(2,128)(2,1)} %reshape.91), calls=%async_computation | async-start | bytes 262144 | tf_op jit(solution)/shard_map/all_to_all | solution.py:98
  92.4 19.8 %all-to-all-start.3 = ((bf16[16,2,2048]{2,1,0:T(2,128)(2,1)}), bf16[16,2,2048]{2,1,0:T(2,128)(2,1)S(1)}, u32[]{:S(2)}, u32[]{:S(2)}) async-start(bf16[16,2,2048]{2,1,0:T(2,128)(2,1)} %reshape.97), calls=%async_computation.3 | async-start | bytes 262144 | tf_op jit(solution)/shard_map/all_to_all | solution.py:147
  112.2 12.3 %all-to-all-start.2 = ((bf16[16,2,2048]{2,1,0:T(2,128)(2,1)}), bf16[16,2,2048]{2,1,0:T(2,128)(2,1)S(1)}, u32[]{:S(2)}, u32[]{:S(2)}) async-start(bf16[16,2,2048]{2,1,0:T(2,128)(2,1)} %reshape.95), calls=%async_computation.2 | async-start | bytes 262144 | tf_op jit(solution)/shard_map/all_to_all | solution.py:140
  115.6 45.1 %all-gather.2.cloned.1.call-start = ((), (), s32[]{:S(2)}) async-start(), calls=%async_computation.4 | async-start | bytes 2228224 | tf_op jit(solution)/shard_map/all_gather | solution.py:12
Sparse Core Ops, SparseCore 0:
  128.6 32.0 all-gather.1
